TPU v7x, 512 devices: a whole 4x8x8 slice. The times are simulated.
512 devices in a mesh: sp: 32 (over z, x), tp: 16 (over y, core).
Axes of the slice: x: 4, y: 8, z: 8, core: 2. Of those that a mesh axis runs over, the one named last changes fastest.
Arguments:
- glu_value: bfloat16 [1024, 8192], P('tp', 'sp')
- glu_gate: bfloat16 [1024, 8192], P('tp', 'sp'), may hold values from -8 to 8
- conv_taps: float32 [1024, 31], P('tp'), may hold values from -1 to 1
- norm_gain: float32 [1024], P('tp'), may hold values from 0.1 to 1.9
- out_proj: bfloat16 [1024, 2048], P(None, 'tp'), may hold values from -0.1875 to 0.1875
- resid: bfloat16 [8192, 2048], P('sp', 'tp'), may hold values from -6 to 6
- expert_ids: int32 [8192, 2], P('sp'), may hold values from 0 to 31, all different within a row; in each aligned block of 256 rows (0 to 255, 256 to 511, ...) at most 32 rows name the same one
- route_logits: float32 [8192, 2], P('sp'), may hold values from -8 to 8
- group_prob: float32 [8192], P('sp'), may hold values from 0.2 to 1
- w_gate: bfloat16 [32, 2048, 4096], P('sp', None, 'tp'), may hold values from -0.125 to 0.125
- w_up: bfloat16 [32, 2048, 4096], P('sp', None, 'tp'), may hold values from -0.125 to 0.125
- w_down: bfloat16 [32, 4096, 2048], P('sp', None, 'tp'), may hold values from -0.09375 to 0.09375
Outputs:
- layer_out: bfloat16 [8192, 2048], P('sp', 'tp')
Inputs may be any that keep to these rules, and one draw needn't show every extreme that they name: `expert_ids`: each row names 2 different experts. In each aligned block of 256 rows (the rows of one index of sp) no expert is named by more than 32 rows, a bound that some block reaches.
All inputs are finite; a program needn't handle non-finite values.
Results may differ from a plain program's by a relative error of at most 0.0061.
Values may be sent and summed in bfloat16 or wider, within the bound.
A program may use at most 64 MiB of HBM per device.

v0:
```python
import jax
import jax.numpy as jnp
from jax import lax
from jax.sharding import PartitionSpec as P


def from_behind(block, axis, distance):
    devices = range(lax.axis_size(axis))
    route = [(i - distance, i) for i in devices if i - distance in devices]
    return lax.ppermute(block, axis, route)


def from_everyone(shard, axis):
    copies = jnp.broadcast_to(shard, (lax.axis_size(axis), *shard.shape))
    return lax.all_to_all(copies, axis, split_axis=0, concat_axis=0, tiled=True)


def of_everyone(shard, axis):
    everything = from_everyone(shard, axis)
    return jnp.sum(everything, axis=0)


def packed_total(arrays, axis):
    ends = [0]
    for a in arrays:
        ends.append(ends[-1] + a.size)
    subtotal = of_everyone(jnp.concatenate([a.ravel() for a in arrays]), axis)
    return tuple((subtotal[b:e].reshape(a.shape) for a, b, e in zip(arrays, ends, ends[1:])))


def per_device(
    glu_value,
    glu_gate,
    conv_taps,
    norm_gain,
    out_proj,
    resid,
    expert_ids,
    route_logits,
    group_prob,
    w_gate,
    w_up,
    w_down,
):
    local_tokens = glu_value.shape[1]
    tap_count = conv_taps.shape[1]
    channels = glu_value.shape[0] * lax.axis_size("tp")
    gated = (glu_value.astype(jnp.float32) * jax.nn.sigmoid(glu_gate.astype(jnp.float32))).astype(
        jnp.bfloat16
    )
    history = from_behind(gated[:, local_tokens - (tap_count - 1) :], "sp", 1)
    padded = jnp.concatenate([history, gated], axis=1).astype(jnp.float32)
    filtered = jnp.zeros(gated.shape, jnp.float32)
    for offset in range(tap_count):
        filtered = (
            filtered + conv_taps[:, offset : offset + 1] * padded[:, offset : offset + local_tokens]
        )
    total_one, total_two = packed_total(
        (jnp.sum(filtered, axis=0), jnp.sum(filtered * filtered, axis=0)), "tp"
    )
    mean = total_one / channels
    var = total_two / channels - mean * mean
    normed = (filtered - mean[None, :]) * lax.rsqrt(var[None, :] + 1e-05) * norm_gain[:, None]
    activated = jax.nn.silu(normed).astype(jnp.bfloat16)
    weights = out_proj
    projected = lax.dot_general(
        lax.all_gather(activated, "tp", axis=0, tiled=True),
        weights,
        (((0,), (0,)), ((), ())),
        preferred_element_type=jnp.float32,
    )
    mixed = (resid.astype(jnp.float32) + projected).astype(jnp.bfloat16)
    experts = lax.axis_size("sp")
    capacity = 4 * local_tokens // experts
    flat_ids = expert_ids.reshape(-1)
    onehot = (flat_ids[:, None] == jnp.arange(experts, dtype=jnp.int32)[None, :]).astype(jnp.int32)
    rank = jnp.sum(jnp.cumsum(onehot, axis=0) * onehot, axis=1) - 1
    slot = flat_ids * capacity + rank
    token_of = jnp.arange(flat_ids.shape[0], dtype=jnp.int32) // expert_ids.shape[1]
    table = jnp.zeros((experts * capacity,), jnp.int32).at[slot].set(token_of)
    filled = jnp.zeros((experts * capacity,), jnp.bool_).at[slot].set(True)
    route_weight = (group_prob[:, None] * jax.nn.softmax(route_logits, axis=-1)).reshape(-1)
    outgoing = jnp.where(
        filled[:, None], jnp.take(mixed, table, axis=0), jnp.zeros((), jnp.bfloat16)
    )
    outgoing = outgoing.reshape(experts, capacity, mixed.shape[1])
    rows = lax.all_gather(
        lax.all_to_all(outgoing, "sp", split_axis=0, concat_axis=0, tiled=True),
        "tp",
        axis=2,
        tiled=True,
    )
    sources, count, width = rows.shape
    flat_rows = rows.reshape(sources * count, width)
    gate_part = jnp.dot(flat_rows, w_gate[0], preferred_element_type=jnp.float32)
    up_part = jnp.dot(flat_rows, w_up[0], preferred_element_type=jnp.float32)
    hidden = (jax.nn.silu(gate_part) * up_part).astype(jnp.bfloat16)
    weights = w_down[0]
    expert_out = jnp.dot(
        lax.all_gather(hidden, "tp", axis=1, tiled=True),
        weights,
        preferred_element_type=jnp.float32,
    )
    results = expert_out.astype(jnp.bfloat16).reshape(sources, count, w_down.shape[2])
    returned = lax.all_to_all(results, "sp", split_axis=0, concat_axis=0, tiled=True)
    flat_back = returned.reshape(experts * capacity, returned.shape[2])
    picked = jnp.take(flat_back, slot, axis=0).astype(jnp.float32) * route_weight[:, None]
    routed = jnp.sum(picked.reshape(local_tokens, expert_ids.shape[1], flat_back.shape[1]), axis=1)
    return (mixed.astype(jnp.float32) + routed).astype(jnp.bfloat16)


def solution(mesh):
    return jax.shard_map(
        per_device,
        mesh=mesh,
        in_specs=(
            P("tp", "sp"),
            P("tp", "sp"),
            P("tp", None),
            P("tp"),
            P(None, "tp"),
            P("sp", "tp"),
            P("sp", None),
            P("sp", None),
            P("sp"),
            P("sp", None, "tp"),
            P("sp", None, "tp"),
            P("sp", None, "tp"),
        ),
        out_specs=P("sp", "tp"),
        check_vma=False,
    )
```

profile of v0, /device:TPU:8, one launch (start us, length us, event | category | flops | bytes accessed | tf_op | source)
XLA Modules:
  0.0 238.1 jit_solution(12596920624349899466)
XLA Ops:
  6.5 0.0 copy-start
  6.5 0.0 copy-start.1
  6.5 0.0 copy-start.2
  6.5 0.9 multiply_convert_fusion.1
  7.5 0.1 slice.272
  7.5 3.4 %collective-permute-start = (bf16[64,30]{1,0:T(8,128)(2,1)S(1)}, bf16[64,30]{1,0:T(8,128)(2,1)S(1)}, u32[]{:S(2)}, u32[]{:S(2)}) collective-permute-start(bf16[64,30]{1,0:T(8,128)(2,1)S(1)} %slice.272), channel_id=1, source_target_pairs={{0,16},{16,32},{32,48},{48,64},{64,80},{80,96},{96,112},{112,128},... | collective-permute-start | bytes 11528 | tf_op jit(solution)/shard_map/ppermute | solution.py:10
  10.9 1.0 slice_bitcast_fusion.30
  11.9 1.0 slice_bitcast_fusion.29
  12.9 0.8 copy.32
  13.7 0.1 eq.26
  13.9 0.1 reshape.114
  14.0 0.7 broadcast_multiply_fusion
  14.7 1.2 reduce-window.6
  15.9 0.2 slice_reduce_fusion
  16.1 0.1 fusion.7
  16.3 0.1 copy.37
  16.4 0.1 mul.489
  16.6 2.4 %scatter_custom_fusion.1 = s32[1024]{0:T(1024)S(1)} fusion(s32[512]{0:T(512)S(1)} %bitcast.102, s32[512]{0:T(512)S(1)} %add_select_fusion, s32[]{:T(128)} %constant.68.clone.1), kind=kCustom, calls=%fused_computation.106 | custom fusion | bytes 4100 | tf_op jit(solution)/shard_map/scatter | solution.py:80
  19.0 0.0 collective-permute-done
  19.0 0.1 maximum_convert_fusion
  19.1 0.9 fusion.48
  20.0 0.6 broadcast_in_dim.60
  20.7 7.6 %all-to-all-start = ((f32[16,1,512]{2,1,0:T(1,128)}), f32[16,1,512]{2,1,0:T(1,128)S(1)}, u32[]{:S(2)}, u32[]{:S(2)}) async-start(f32[16,1,512]{2,1,0:T(1,128)} %broadcast_in_dim.60), calls=%async_computation | async-start | bytes 65536 | tf_op jit(solution)/shard_map/all_to_all | solution.py:15
  28.2 0.0 all-gather.3.cloned.1.call-start
  28.3 0.1 broadcast_in_dim.67
  28.4 2.4 %scatter_custom_fusion = pred[1024]{0:T(1024)(128)(4,1)S(1)} fusion(s32[512]{0:T(512)S(1)} %bitcast.103, pred[512]{0:T(512)(128)(4,1)S(1)} %broadcast.121, pred[]{:T(512)} %constant.72.clone.1), kind=kCustom, calls=%fused_computation.109 | custom fusion | bytes 1025 | tf_op jit(solution)/shard_map/scatter | solution.py:81
  30.8 0.1 broadcast_in_dim.64
  30.9 3.6 %all-to-all-done = f32[16,1,512]{2,1,0:T(1,128)S(1)} async-done(((f32[16,1,512]{2,1,0:T(1,128)}), f32[16,1,512]{2,1,0:T(1,128)S(1)}, u32[]{:S(2)}, u32[]{:S(2)}) %all-to-all-start) | async-done | bytes 32800 | tf_op jit(solution)/shard_map/all_to_all | solution.py:15
  34.6 0.8 multiply_convert_fusion
  35.3 17.0 %all_gather.9 = bf16[1024,256]{1,0:T(8,128)(2,1)S(1)} all-gather(bf16[64,256]{1,0:T(8,128)(2,1)S(1)} %multiply_convert_fusion), channel_id=1, replica_groups=mesh['sp'=32,'tp'=16] {'tp'}, dimensions={0}, use_global_device_ids=true | all-gather | bytes 557056 | tf_op jit(solution)/shard_map/all_gather | solution.py:67
  52.4 0.0 copy-done.1
  52.4 0.0 copy-done.2
  52.4 0.3 fusion.1
  52.7 3.2 %gather_fusion = bf16[1024,128]{1,0:T(8,128)(2,1)S(1)} fusion(bf16[256,128]{1,0:T(8,128)(2,1)S(1)} %fusion.1, s32[1024]{0:T(1024)S(1)} %fusion.39), kind=kCustom, calls=%fused_computation | custom fusion | bytes 528384 | tf_op jit(solution)/shard_map/jit(_take)/gather | solution.py:84
  55.9 0.3 select_select_fusion
  56.3 0.0 copy-start.7
  56.3 26.5 %all_to_all.16 = bf16[32,32,128]{2,1,0:T(8,128)(2,1)} all-to-all(bf16[32,32,128]{2,1,0:T(8,128)(2,1)S(1)} %select_select_fusion), channel_id=1, replica_groups=mesh['sp'=32,'tp'=16] {'sp'}, dimensions={0} | all-to-all | bytes 524288 | tf_op jit(solution)/shard_map/all_to_all | solution.py:88
  82.7 0.0 all-gather.3.cloned.1.call-update
  82.8 0.0 all-gather.5.cloned.1.call-start
  82.8 43.3 %all-gather.3.cloned.1.call-done = bf16[32,32,2048]{2,1,0:T(8,128)(2,1)} async-done(((bf16[32,32,128]{2,1,0:T(8,128)(2,1)}), bf16[32,32,2048]{2,1,0:T(8,128)(2,1)}) %all-gather.3.cloned.1.call-update) | async-done | bytes 4194320 | tf_op jit(solution)/shard_map/all_gather | solution.py:87
  126.1 0.0 copy-start.6
  126.1 0.0 copy-done
  126.1 3.6 %fusion.4 = f32[1024,256]{1,0:T(8,128)S(1)} fusion(bf16[1024,2048]{1,0:T(8,128)(2,1)} %bitcast.105, bf16[1,2048,256]{2,1,0:T(8,128)(2,1)S(1)} %copy-done), kind=kOutput, calls=%fused_computation.11 | convolution fusion | flops 1073741824 | bytes 6291456 | tf_op jit(solution)/shard_map/dot_general | solution.py:95
  129.7 0.0 copy-done.7
  129.8 0.0 copy-done.6
  129.8 2.1 fusion
  131.9 0.0 all-gather.5.cloned.1.call-update
  131.9 0.1 sub.37
  132.1 0.1 copy.35
  132.2 0.0 copy-start.3
  132.2 0.0 copy-start.4
  132.2 0.0 copy-start.5
  132.2 66.1 %all-gather.5.cloned.1.call-done = bf16[1024,4096]{1,0:T(8,128)(2,1)} async-done(((bf16[1024,256]{1,0:T(8,128)(2,1)}), bf16[1024,4096]{1,0:T(8,128)(2,1)}) %all-gather.5.cloned.1.call-update) | async-done | bytes 8388624 | tf_op jit(solution)/shard_map/all_gather | solution.py:100
  198.3 6.6 %convolution_convert_fusion = bf16[1024,128]{1,0:T(8,128)(2,1)} fusion(bf16[1024,4096]{1,0:T(8,128)(2,1)} %all-gather.5.cloned.1.call-done, bf16[1,4096,128]{2,1,0:T(8,128)(2,1)} %param.23), kind=kOutput, calls=%fused_computation.6 | convolution fusion | flops 1073872896 | bytes 9699328 | tf_op jit(solution)/shard_map/dot_general | solution.py:99
  204.9 9.4 %all-to-all-start.2 = ((bf16[32,32,128]{2,1,0:T(8,128)(2,1)}), bf16[32,32,128]{2,1,0:T(8,128)(2,1)S(1)}, u32[]{:S(2)}, u32[]{:S(2)}) async-start(bf16[32,32,128]{2,1,0:T(8,128)(2,1)} %bitcast.39), calls=%async_computation.2 | async-start | bytes 524288 | tf_op jit(solution)/shard_map/all_to_all | solution.py:105
  214.3 0.0 copy-done.3
  214.4 0.2 copy.36
  214.6 0.0 copy-done.4
  214.6 0.0 copy-done.5
  214.6 0.1 copy.38
  214.8 13.0 %all-to-all-done.2 = bf16[32,32,128]{2,1,0:T(8,128)(2,1)S(1)} async-done(((bf16[32,32,128]{2,1,0:T(8,128)(2,1)}), bf16[32,32,128]{2,1,0:T(8,128)(2,1)S(1)}, u32[]{:S(2)}, u32[]{:S(2)}) %all-to-all-start.2) | async-done | bytes 262176 | tf_op jit(solution)/shard_map/all_to_all | solution.py:105
  227.8 1.3 gather_fusion.1
  229.1 1.5 multiply_reduce_fusion
  230.6 0.7 add_convert_fusion
  (17 shorter events, 0.2 us)
Async XLA Ops:
  6.5 119.6 %copy-start = (bf16[1,2048,256]{2,1,0:T(8,128)(2,1)S(1)}, bf16[1,2048,256]{2,1,0:T(8,128)(2,1)}, u32[]{:S(2)}) copy-start(bf16[1,2048,256]{2,1,0:T(8,128)(2,1)} %param.21) | copy-start | bytes 3145732
  6.5 45.8 %copy-start.1 = (bf16[1024,128]{1,0:T(8,128)(2,1)S(1)}, bf16[1024,128]{1,0:T(8,128)(2,1)}, u32[]{:S(2)}) copy-start(bf16[1024,128]{1,0:T(8,128)(2,1)} %param.16) | copy-start | bytes 786436
  6.5 45.8 %copy-start.2 = (bf16[256,128]{1,0:T(8,128)(2,1)S(1)}, bf16[256,128]{1,0:T(8,128)(2,1)}, u32[]{:S(2)}) copy-start(bf16[256,128]{1,0:T(8,128)(2,1)} %param.17) | copy-start | bytes 196612
  7.5 11.5 %collective-permute-start = (bf16[64,30]{1,0:T(8,128)(2,1)S(1)}, bf16[64,30]{1,0:T(8,128)(2,1)S(1)}, u32[]{:S(2)}, u32[]{:S(2)}) collective-permute-start(bf16[64,30]{1,0:T(8,128)(2,1)S(1)} %slice.272), channel_id=1, source_target_pairs={{0,16},{16,32},{32,48},{48,64},{64,80},{80,96},{96,112},{112,128},... | collective-permute-start | bytes 11528 | tf_op jit(solution)/shard_map/ppermute | solution.py:10
  20.7 13.9 %all-to-all-start = ((f32[16,1,512]{2,1,0:T(1,128)}), f32[16,1,512]{2,1,0:T(1,128)S(1)}, u32[]{:S(2)}, u32[]{:S(2)}) async-start(f32[16,1,512]{2,1,0:T(1,128)} %broadcast_in_dim.60), calls=%async_computation | async-start | bytes 65536 | tf_op jit(solution)/shard_map/all_to_all | solution.py:15
  28.2 97.9 %all-gather.3.cloned.1.call-start = ((), (), s32[]{:S(2)}) async-start(), calls=%async_computation.3 | async-start | bytes 4456448 | tf_op jit(solution)/shard_map/all_gather | solution.py:87
  56.3 73.5 %copy-start.7 = (bf16[1,2048,256]{2,1,0:T(8,128)(2,1)S(1)}, bf16[1,2048,256]{2,1,0:T(8,128)(2,1)}, u32[]{:S(2)}) copy-start(bf16[1,2048,256]{2,1,0:T(8,128)(2,1)} %param.22) | copy-start | bytes 3145732
  82.8 115.5 %all-gather.5.cloned.1.call-start = ((), (), s32[]{:S(2)}) async-start(), calls=%async_computation.4 | async-start | bytes 8912896 | tf_op jit(solution)/shard_map/all_gather | solution.py:100
  126.1 3.6 %copy-start.6 = (bf16[32,32,2048]{2,1,0:T(8,128)(2,1)S(1)}, bf16[32,32,2048]{2,1,0:T(8,128)(2,1)}, u32[]{:S(2)}) copy-start(bf16[32,32,2048]{2,1,0:T(8,128)(2,1)} %all-gather.3.cloned.1.call-done) | copy-start | bytes 12582916
  132.2 82.2 %copy-start.3 = (s32[256,2]{0,1:T(2,128)S(1)}, s32[256,2]{0,1:T(2,128)}, u32[]{:S(2)}) copy-start(s32[256,2]{0,1:T(2,128)} %param.18) | copy-start | bytes 6148
  132.2 82.4 %copy-start.4 = (f32[256,2]{0,1:T(2,128)S(1)}, f32[256,2]{0,1:T(2,128)}, u32[]{:S(2)}) copy-start(f32[256,2]{0,1:T(2,128)} %param.19) | copy-start | bytes 6148
  132.2 82.5 %copy-start.5 = (f32[256]{0:T(256)S(1)}, f32[256]{0:T(256)}, u32[]{:S(2)}) copy-start(f32[256]{0:T(256)} %param.20) | copy-start | bytes 3076
  204.9 22.8 %all-to-all-start.2 = ((bf16[32,32,128]{2,1,0:T(8,128)(2,1)}), bf16[32,32,128]{2,1,0:T(8,128)(2,1)S(1)}, u32[]{:S(2)}, u32[]{:S(2)}) async-start(bf16[32,32,128]{2,1,0:T(8,128)(2,1)} %bitcast.39), calls=%async_computation.2 | async-start | bytes 524288 | tf_op jit(solution)/shard_map/all_to_all | solution.py:105
Sparse Core Ops, SparseCore 0:
  82.9 43.2 all-gather.2
  132.1 66.1 all-gather.4
where the time goes:
time: 239 us; the launch traced here: 238 us
  waiting for transfers between devices  126 us (53%)
  blocking collectives  43.5 us (18%)
  starting transfers between devices  20.4 us (9%)
  local copies, waits for them, and re-layouts  14.4 us (6%)
  between operations  13.7 us (6%)
  matrix products  12.7 us (5%)
  other arithmetic  7.23 us (3%)
    all_gather x1, waiting for transfers between devices, per_device(): lax.all_gather(hidden, 'tp', axis=1, tiled=True)  66.1 us
    all_gather x1, waiting for transfers between devices, per_device(): lax.all_gather(lax.all_to_all(outgoing, 'sp', split_axis=0, concat_axis=0...  43.3 us
    all_to_all x1, blocking collectives, per_device(): lax.all_to_all(outgoing, 'sp', split_axis=0, concat_axis=0, tiled=True)  26.5 us
    all_gather x1, blocking collectives, per_device(): lax.all_gather(activated, 'tp', axis=0, tiled=True)  17 us
    all_to_all x1, waiting for transfers between devices, per_device(): lax.all_to_all(results, 'sp', split_axis=0, concat_axis=0, tiled=True)  13 us
    all_to_all x1, starting transfers between devices, per_device(): lax.all_to_all(results, 'sp', split_axis=0, concat_axis=0, tiled=True)  9.41 us
    all_to_all x1, starting transfers between devices, from_everyone(): return lax.all_to_all(copies, axis, split_axis=0, concat_axis=0, tiled=True)  7.56 us
    dot_general x1, matrix products, per_device(): jnp.dot(lax.all_gather(hidden, 'tp', axis=1, tiled=True), weights, prefer...  6.65 us
  transfers between devices with their start and end apart: 5, of which 4 were waited for; matrix products, arithmetic and copies ran while one was open for 5% of the time, Pallas kernels for 0%

commit v1 on v0

--- a/solution.py
+++ b/solution.py
@@ -2,6 +2,16 @@
 import jax.numpy as jnp
 from jax import lax
 from jax.sharding import PartitionSpec as P
+
+
+def resolve_the_files(sheet, row_axis="tp"):
+    high = jnp.concatenate(
+        lax.all_to_all(
+            jnp.stack(tuple((sheet for _ in range(lax.psum(1, row_axis)))), 0), row_axis, 0, 0
+        ),
+        1,
+    )
+    return high
 
 
 def from_behind(block, axis, distance):
@@ -96,11 +106,7 @@
     up_part = jnp.dot(flat_rows, w_up[0], preferred_element_type=jnp.float32)
     hidden = (jax.nn.silu(gate_part) * up_part).astype(jnp.bfloat16)
     weights = w_down[0]
-    expert_out = jnp.dot(
-        lax.all_gather(hidden, "tp", axis=1, tiled=True),
-        weights,
-        preferred_element_type=jnp.float32,
-    )
+    expert_out = jnp.dot(resolve_the_files(hidden), weights, preferred_element_type=jnp.float32)
     results = expert_out.astype(jnp.bfloat16).reshape(sources, count, w_down.shape[2])
     returned = lax.all_to_all(results, "sp", split_axis=0, concat_axis=0, tiled=True)
     flat_back = returned.reshape(experts * capacity, returned.shape[2])

time: 239 us -> 366 us (1.53)
  the two profiles are of different devices: /device:TPU:8 before, /device:TPU:24 now
where the time goes in v1:
time: 366 us; the launch traced here: 365 us
  waiting for transfers between devices  243 us (66%)
  blocking collectives  43.1 us (12%)
  starting transfers between devices  27.4 us (7%)
  local copies, waits for them, and re-layouts  18.9 us (5%)
  between operations  13.7 us (4%)
  matrix products  11.7 us (3%)
  other arithmetic  7.23 us (2%)
    all_to_all x1, waiting for transfers between devices, resolve_the_files(): lax.all_to_all(jnp.stack(tuple((sheet for _ in range(lax.psum(1, row_axis...  183 us
    all_gather x1, waiting for transfers between devices, per_device(): lax.all_gather(lax.all_to_all(outgoing, 'sp', split_axis=0, concat_axis=0...  44.7 us
    all_to_all x1, blocking collectives, per_device(): lax.all_to_all(outgoing, 'sp', split_axis=0, concat_axis=0, tiled=True)  26.5 us
    all_gather x1, blocking collectives, per_device(): lax.all_gather(activated, 'tp', axis=0, tiled=True)  16.6 us
    all_to_all x1, waiting for transfers between devices, per_device(): lax.all_to_all(results, 'sp', split_axis=0, concat_axis=0, tiled=True)  12.8 us
    all_to_all x1, starting transfers between devices, per_device(): lax.all_to_all(results, 'sp', split_axis=0, concat_axis=0, tiled=True)  9.23 us
    all_to_all x1, starting transfers between devices, resolve_the_files(): lax.all_to_all(jnp.stack(tuple((sheet for _ in range(lax.psum(1, row_axis...  7.44 us
    all_to_all x1, starting transfers between devices, from_everyone(): return lax.all_to_all(copies, axis, split_axis=0, concat_axis=0, tiled=True)  7.34 us
  transfers between devices with their start and end apart: 5, of which 4 were waited for; matrix products, arithmetic and copies ran while one was open for 3% of the time, Pallas kernels for 0%

profile of v1, /device:TPU:24, one launch (start us, length us, event | category | flops | bytes accessed | tf_op | source)
XLA Modules:
  0.0 364.9 jit_solution(3360036895538678196)
XLA Ops:
  6.5 0.0 copy-start
  6.5 0.0 copy-start.1
  6.5 0.9 multiply_convert_fusion.1
  7.5 0.1 slice.272
  7.5 3.4 collective-permute-start
  10.9 1.0 slice_bitcast_fusion.30
  11.9 1.0 slice_bitcast_fusion.29
  12.9 0.8 copy.35
  13.7 0.1 eq.26
  13.9 0.1 reshape.122
  14.0 0.7 broadcast_multiply_fusion
  14.7 1.2 reduce-window.6
  15.9 0.2 slice_reduce_fusion
  16.1 0.1 fusion.7
  16.3 0.1 copy.40
  16.4 0.1 mul.489
  16.6 2.4 scatter_custom_fusion.1
  19.0 0.0 collective-permute-done
  19.0 0.1 maximum_convert_fusion
  19.1 0.9 fusion.48
  20.0 0.6 broadcast_in_dim.60
  20.7 7.3 %all-to-all-start = ((f32[16,1,512]{2,1,0:T(1,128)}), f32[16,1,512]{2,1,0:T(1,128)S(1)}, u32[]{:S(2)}, u32[]{:S(2)}) async-start(f32[16,1,512]{2,1,0:T(1,128)} %broadcast_in_dim.60), calls=%async_computation | async-start | bytes 65536 | tf_op jit(solution)/shard_map/all_to_all | solution.py:25
  28.0 0.0 all-gather.2.cloned.1.call-start
  28.0 0.1 broadcast_in_dim.67
  28.1 2.4 scatter_custom_fusion
  30.6 0.1 broadcast_in_dim.64
  30.7 1.9 all-to-all-done
  32.7 0.8 multiply_convert_fusion
  33.4 16.6 %all_gather.6 = bf16[1024,256]{1,0:T(8,128)(2,1)S(1)} all-gather(bf16[64,256]{1,0:T(8,128)(2,1)S(1)} %multiply_convert_fusion), channel_id=1, replica_groups=mesh['sp'=32,'tp'=16] {'tp'}, dimensions={0}, use_global_device_ids=true | all-gather | bytes 557056 | tf_op jit(solution)/shard_map/all_gather | solution.py:77
  50.0 0.0 copy-done.1
  50.0 0.0 copy-done.2
  50.0 0.3 fusion.1
  50.4 3.2 gather_fusion
  53.6 0.3 select_select_fusion
  53.9 0.0 copy-start.7
  54.0 26.5 %all_to_all.21 = bf16[32,32,128]{2,1,0:T(8,128)(2,1)} all-to-all(bf16[32,32,128]{2,1,0:T(8,128)(2,1)S(1)} %select_select_fusion), channel_id=1, replica_groups=mesh['sp'=32,'tp'=16] {'sp'}, dimensions={0} | all-to-all | bytes 524288 | tf_op jit(solution)/shard_map/all_to_all | solution.py:98
  80.4 0.0 all-gather.2.cloned.1.call-update
  80.4 44.7 %all-gather.2.cloned.1.call-done = bf16[32,32,2048]{2,1,0:T(8,128)(2,1)} async-done(((bf16[32,32,128]{2,1,0:T(8,128)(2,1)}), bf16[32,32,2048]{2,1,0:T(8,128)(2,1)}) %all-gather.2.cloned.1.call-update) | async-done | bytes 4194320 | tf_op jit(solution)/shard_map/all_gather | solution.py:97
  125.2 0.0 copy-start.6
  125.2 0.0 copy-done
  125.2 3.6 fusion.4
  128.8 0.0 copy-done.7
  128.8 0.0 copy-done.6
  128.8 1.3 fusion
  130.1 0.2 copy.41
  130.3 4.3 %stack.2 = bf16[16,1024,256]{1,2,0:T(8,128)(2,1)} broadcast(bf16[1024,256]{0,1:T(8,128)(2,1)S(1)} %copy.41), dimensions={1,2} | broadcast | bytes 8912896 | tf_op jit(solution)/shard_map/stack | solution.py:10
  134.6 0.0 copy-start.8
  134.6 7.4 %all-to-all-start.2 = ((bf16[16,1024,256]{1,2,0:T(8,128)(2,1)}), bf16[16,1024,256]{1,2,0:T(8,128)(2,1)}, u32[]{:S(2)}, u32[]{:S(2)}) async-start(bf16[16,1024,256]{1,2,0:T(8,128)(2,1)} %stack.2), calls=%async_computation.2 | async-start | bytes 16777216 | tf_op jit(solution)/shard_map/all_to_all | solution.py:9
  142.0 0.1 sub.37
  142.2 0.1 copy.38
  142.2 183.4 %all-to-all-done.2 = bf16[16,1024,256]{1,2,0:T(8,128)(2,1)} async-done(((bf16[16,1024,256]{1,2,0:T(8,128)(2,1)}), bf16[16,1024,256]{1,2,0:T(8,128)(2,1)}, u32[]{:S(2)}, u32[]{:S(2)}) %all-to-all-start.2) | async-done | bytes 8388640 | tf_op jit(solution)/shard_map/all_to_all | solution.py:9
  325.6 0.0 copy-done.8
  325.6 0.0 copy-start.4
  325.6 6.5 %convolution_convert_fusion = bf16[1024,128]{1,0:T(8,128)(2,1)} fusion(bf16[1024,4096]{0,1:T(8,128)(2,1)} %bitcast.39, bf16[1,4096,128]{2,1,0:T(8,128)(2,1)S(1)} %copy-done.8), kind=kOutput, calls=%fused_computation.6 | convolution fusion | flops 1073872896 | bytes 9699328 | tf_op jit(solution)/shard_map/dot_general | solution.py:109
  332.2 9.2 %all-to-all-start.3 = ((bf16[32,32,128]{2,1,0:T(8,128)(2,1)}), bf16[32,32,128]{2,1,0:T(8,128)(2,1)S(1)}, u32[]{:S(2)}, u32[]{:S(2)}) async-start(bf16[32,32,128]{2,1,0:T(8,128)(2,1)} %bitcast.41), calls=%async_computation.3 | async-start | bytes 524288 | tf_op jit(solution)/shard_map/all_to_all | solution.py:111
  341.4 0.0 copy-done.3
  341.4 0.2 copy.39
  341.6 0.0 copy-done.4
  341.7 0.0 copy-done.5
  341.7 0.1 copy.42
  341.9 12.8 %all-to-all-done.3 = bf16[32,32,128]{2,1,0:T(8,128)(2,1)S(1)} async-done(((bf16[32,32,128]{2,1,0:T(8,128)(2,1)}), bf16[32,32,128]{2,1,0:T(8,128)(2,1)S(1)}, u32[]{:S(2)}, u32[]{:S(2)}) %all-to-all-start.3) | async-done | bytes 262176 | tf_op jit(solution)/shard_map/all_to_all | solution.py:111
  354.6 1.3 gather_fusion.1
  356.0 1.5 multiply_reduce_fusion
  357.4 0.6 add_convert_fusion
  (20 shorter events, 0.2 us)
Async XLA Ops:
  6.5 118.6 %copy-start = (bf16[1,2048,256]{2,1,0:T(8,128)(2,1)S(1)}, bf16[1,2048,256]{2,1,0:T(8,128)(2,1)}, u32[]{:S(2)}) copy-start(bf16[1,2048,256]{2,1,0:T(8,128)(2,1)} %param.21) | copy-start | bytes 3145732
  6.5 43.5 %copy-start.1 = (bf16[1024,128]{1,0:T(8,128)(2,1)S(1)}, bf16[1024,128]{1,0:T(8,128)(2,1)}, u32[]{:S(2)}) copy-start(bf16[1024,128]{1,0:T(8,128)(2,1)} %param.16) | copy-start | bytes 786436
  6.5 43.5 %copy-start.2 = (bf16[256,128]{1,0:T(8,128)(2,1)S(1)}, bf16[256,128]{1,0:T(8,128)(2,1)}, u32[]{:S(2)}) copy-start(bf16[256,128]{1,0:T(8,128)(2,1)} %param.17) | copy-start | bytes 196612
  7.5 11.5 %collective-permute-start = (bf16[64,30]{1,0:T(8,128)(2,1)S(1)}, bf16[64,30]{1,0:T(8,128)(2,1)S(1)}, u32[]{:S(2)}, u32[]{:S(2)}) collective-permute-start(bf16[64,30]{1,0:T(8,128)(2,1)S(1)} %slice.272), channel_id=1, source_target_pairs={{0,16},{16,32},{32,48},{48,64},{64,80},{80,96},{96,112},{112,128},... | collective-permute-start | bytes 11528 | tf_op jit(solution)/shard_map/ppermute | solution.py:20
  20.7 12.0 %all-to-all-start = ((f32[16,1,512]{2,1,0:T(1,128)}), f32[16,1,512]{2,1,0:T(1,128)S(1)}, u32[]{:S(2)}, u32[]{:S(2)}) async-start(f32[16,1,512]{2,1,0:T(1,128)} %broadcast_in_dim.60), calls=%async_computation | async-start | bytes 65536 | tf_op jit(solution)/shard_map/all_to_all | solution.py:25
  28.0 97.2 %all-gather.2.cloned.1.call-start = ((), (), s32[]{:S(2)}) async-start(), calls=%async_computation.4 | async-start | bytes 4456448 | tf_op jit(solution)/shard_map/all_gather | solution.py:97
  53.9 74.8 %copy-start.7 = (bf16[1,2048,256]{2,1,0:T(8,128)(2,1)S(1)}, bf16[1,2048,256]{2,1,0:T(8,128)(2,1)}, u32[]{:S(2)}) copy-start(bf16[1,2048,256]{2,1,0:T(8,128)(2,1)} %param.22) | copy-start | bytes 3145732
  125.2 3.6 copy-start.6
  134.6 191.1 %copy-start.8 = (bf16[1,4096,128]{2,1,0:T(8,128)(2,1)S(1)}, bf16[1,4096,128]{2,1,0:T(8,128)(2,1)}, u32[]{:S(2)}) copy-start(bf16[1,4096,128]{2,1,0:T(8,128)(2,1)} %param.23) | copy-start | bytes 3145732
  134.6 191.1 %all-to-all-start.2 = ((bf16[16,1024,256]{1,2,0:T(8,128)(2,1)}), bf16[16,1024,256]{1,2,0:T(8,128)(2,1)}, u32[]{:S(2)}, u32[]{:S(2)}) async-start(bf16[16,1024,256]{1,2,0:T(8,128)(2,1)} %stack.2), calls=%async_computation.2 | async-start | bytes 16777216 | tf_op jit(solution)/shard_map/all_to_all | solution.py:9
  325.6 15.8 %copy-start.3 = (s32[256,2]{0,1:T(2,128)S(1)}, s32[256,2]{0,1:T(2,128)}, u32[]{:S(2)}) copy-start(s32[256,2]{0,1:T(2,128)} %param.18) | copy-start | bytes 6148
  325.6 16.0 %copy-start.4 = (f32[256,2]{0,1:T(2,128)S(1)}, f32[256,2]{0,1:T(2,128)}, u32[]{:S(2)}) copy-start(f32[256,2]{0,1:T(2,128)} %param.19) | copy-start | bytes 6148
  325.6 16.0 %copy-start.5 = (f32[256]{0:T(256)S(1)}, f32[256]{0:T(256)}, u32[]{:S(2)}) copy-start(f32[256]{0:T(256)} %param.20) | copy-start | bytes 3076
  332.2 22.5 %all-to-all-start.3 = ((bf16[32,32,128]{2,1,0:T(8,128)(2,1)}), bf16[32,32,128]{2,1,0:T(8,128)(2,1)S(1)}, u32[]{:S(2)}, u32[]{:S(2)}) async-start(bf16[32,32,128]{2,1,0:T(8,128)(2,1)} %bitcast.41), calls=%async_computation.3 | async-start | bytes 524288 | tf_op jit(solution)/shard_map/all_to_all | solution.py:111
Sparse Core Ops, SparseCore 0:
  80.6 44.5 all-gather.1
